TPU v7x, 32 devices: a whole 2x2x4 slice. The times are simulated.
32 devices in a mesh: sp: 8 (over z, y), tp: 4 (over x, core).
Axes of the slice: x: 2, y: 2, z: 4, core: 2. Of those that a mesh axis runs over, the one named last changes fastest.
Arguments:
- hidden: bfloat16 [3072, 4096], P('sp', 'tp'), may hold values from -6 to 6
- doc_ids: int32 [3072], P('sp'), may hold values from 0 to 3, never falling along the last dimension, each value on 1 to 1536 neighbouring positions
- norm_gain: float32 [3, 4096], replicated, may hold values from 0.1 to 1.9
- w_value: bfloat16 [3, 4096, 2048], P(None, 'sp', 'tp'), may hold values from -0.09375 to 0.09375
- w_gate: bfloat16 [3, 4096, 2048], P(None, 'sp', 'tp'), may hold values from -0.09375 to 0.09375
- conv_taps: float32 [3, 31, 2048], P(None, None, 'tp'), may hold values from -1 to 1
- conv_bias: float32 [3, 2048], P(None, 'tp'), may hold values from -3 to 3
- chan_gain: float32 [3, 2048], P(None, 'tp'), may hold values from 0.1 to 1.9
- chan_bias: float32 [3, 2048], P(None, 'tp'), may hold values from -3 to 3
- w_out: bfloat16 [3, 2048, 4096], P(None, 'sp', 'tp'), may hold values from -0.125 to 0.125
Outputs:
- result: bfloat16 [3072, 4096], P('sp', 'tp')
Inputs may be any that keep to these rules, and one draw needn't show every extreme that they name: `doc_ids`: document numbers never fall along the sequence; each document has 1 to 1536 positions and one has exactly that many.
All inputs are finite; a program needn't handle non-finite values.
Results may differ from a plain program's by a relative error of at most 0.013.
Values may be sent and summed in bfloat16 or wider, within the bound.
A program may use at most 128 MiB of HBM per device.

v0:
```python
import functools
import math

import jax
import jax.numpy as jnp
from jax import lax
from jax.experimental import pallas as pl
from jax.experimental.pallas import tpu as pltpu
from jax.sharding import PartitionSpec as P

MESH = pl.DeviceIdType.MESH
HALO = 32
ROWS = 64


def grid_of(size):
    inner = max(d for d in range(1, math.isqrt(size) + 1) if size % d == 0)
    return size // inner, inner


def kernel(
    dims,
    hid,
    pos,
    ngain,
    wv,
    wg,
    taps,
    cbias,
    cgain,
    chbias,
    wo,
    out,
    wp_buf,
    wo_buf,
    rp_buf,
    ro_buf,
    xg,
    xn,
    mg,
    prod,
    branch,
    glu,
    conv,
    state,
    final,
    tail,
    halo,
    stat,
    stat_out,
    stat_in,
    cols,
    loc_sem,
    z_recv,
    r_recv,
    y_recv,
    z_send,
    y_send,
    h_recv,
    h_send,
    m_recv,
    m_send,
    s_recv,
    s_send,
    t_recv,
    t_send,
    f_sem,
):
    Z, Y, X, T, D, C, LAYERS, WIDTH = dims
    S = 4 * X
    cs, ds_ = C // S, D // S
    parts = 2 * LAYERS
    nx, ny = X - 1, Y - 1

    spi, tpi = lax.axis_index("sp"), lax.axis_index("tp")
    z, y, x, c = spi // Y, spi % Y, tpi // 2, tpi % 2
    zn = z + 1 - 2 * (z % 2)
    zh, ko = z // 2, z % 2
    inner = ((z + 1) // 2) % 2
    h = 1 - inner
    zin = inner * z + h * zn
    zout = h * z + inner * zn
    me = (x * 2 + c) * 2 + h

    def dev(zz, yy, xx, cc):
        return (zz * Y + yy, xx * 2 + cc)

    partner = dev(z, y, x, 1 - c)
    zpeer = dev(zn, y, x, c)
    mid = dev(Z - 1 - z, y, x, c)

    def send(src, dst, ssem, rsem, device):
        pltpu.make_async_remote_copy(
            src_ref=src, dst_ref=dst, send_sem=ssem, recv_sem=rsem,
            device_id=device, device_id_type=MESH,
        ).start()

    def recv_wait(ref, sem):
        pltpu.make_async_remote_copy(
            src_ref=ref, dst_ref=ref, send_sem=sem, recv_sem=sem,
            device_id=partner, device_id_type=MESH,
        ).wait_recv()

    def send_wait(ref, sem):
        pltpu.make_async_remote_copy(
            src_ref=ref, dst_ref=ref, send_sem=sem, recv_sem=sem,
            device_id=partner, device_id_type=MESH,
        ).wait_send()

    def lanes(start, size):
        return pl.ds(pl.multiple_of(start, 128), size)

    def block(q, b):
        return (wo_buf if q % 2 else wp_buf).at[q // 2, b]

    def relay(q, i):
        return (ro_buf if q % 2 else rp_buf).at[q // 2, i]

    def own_pieces(q, half, dst):
        l = q // 2
        if q % 2:
            return [(wo.at[l, :, lanes(half * ds_, ds_)], dst)]
        return [
            (wv.at[l, :, lanes(half * cs, cs)], dst.at[:, pl.ds(0, cs)]),
            (wg.at[l, :, lanes(half * cs, cs)], dst.at[:, pl.ds(cs, cs)]),
        ]

    def own_send(q, half, dst, ssem, rsem, device):
        for src, part in own_pieces(q, half, dst):
            send(src, part, ssem, rsem, device)

    def y_spread(q, zb):
        b = zb * Y + y
        for j in range(1, Y):
            send(block(q, b), block(q, b), y_send.at[q, zb, j - 1], y_recv.at[q, zb, j - 1],
                 dev(z, (y + j) % Y, x, c))

    def start_part(q):
        mine = block(q, z * Y + y)
        own_send(q, 1 - h, mine, z_send.at[q, 0], z_recv.at[q, 0], zpeer)

        @pl.when(inner == 0)
        def _():
            own_send(q, h, relay(q, 1), z_send.at[q, 1], r_recv.at[q, 1], zpeer)

        @pl.when(inner == 1)
        def _():
            own_send(q, 1 - h, relay(q, 0), z_send.at[q, 1], r_recv.at[q, 0], mid)
            own_send(q, h, mine, z_send.at[q, 2], z_recv.at[q, 1], mid)

        for j in range(1, Y):
            own_send(q, h, mine, y_send.at[q, z, j - 1], y_recv.at[q, z, j - 1],
                     dev(z, (y + j) % Y, x, c))
        for src, part in own_pieces(q, h, mine):
            pltpu.make_async_copy(src, part, loc_sem.at[q]).start()

    def event1(q):
        recv_wait(block(q, zn * Y + y), z_recv.at[q, 0])
        y_spread(q, zn)

        @pl.when(inner == 1)
        def _():
            recv_wait(relay(q, 0), r_recv.at[q, 0])
            send(relay(q, 0), block(q, (Z - 1 - z) * Y + y), z_send.at[q, 3], z_recv.at[q, 1], zpeer)

    def event2(q):
        @pl.when(inner == 1)
        def _():
            recv_wait(relay(q, 1), r_recv.at[q, 1])
            send(relay(q, 1), relay(q, 2), z_send.at[q, 4], r_recv.at[q, 2], mid)
            near = block(q, zn * Y + y)
            send(near, near, z_send.at[q, 5], z_recv.at[q, 2], mid)

        zb = Z - 1 - zin
        recv_wait(block(q, zb * Y + y), z_recv.at[q, 1])
        y_spread(q, zb)

    def event3(q):
        @pl.when(inner == 1)
        def _():
            recv_wait(relay(q, 2), r_recv.at[q, 2])
            send(relay(q, 2), block(q, (Z - 1 - zn) * Y + y), z_send.at[q, 6], z_recv.at[q, 2], zpeer)

    def event4(q):
        zb = Z - 1 - zout
        recv_wait(block(q, zb * Y + y), z_recv.at[q, 2])
        y_spread(q, zb)

    def part_ready(q):
        mine = block(q, z * Y + y)
        pltpu.make_async_copy(mine, mine, loc_sem.at[q]).wait()
        for zb in range(Z):
            for j in range(1, Y):
                recv_wait(block(q, zb * Y + (y - j + Y) % Y), y_recv.at[q, zb, j - 1])

    def part_sent(q):
        ref = block(q, 0)
        for zb in range(Z):
            for j in range(1, Y):
                send_wait(ref, y_send.at[q, zb, j - 1])
        send_wait(ref, z_send.at[q, 0])
        send_wait(ref, z_send.at[q, 1])

        @pl.when(inner == 1)
        def _():
            for i in range(2, 7):
                send_wait(ref, z_send.at[q, i])

    class Gather:
        def __init__(self, region, recv, sent, source=None):
            self.region, self.recv, self.sent = region, recv, sent
            self.own = region(x, c, z)
            self.source = self.own if source is None else source

        def xs(self, j):
            return (x - j + X) % X

        def forward(self, ref, i, device):
            send(ref, ref, self.sent.at[i], self.recv.at[i], device)

        def first(self):
            def go(i, device):
                send(self.source, self.own, self.sent.at[i], self.recv.at[i], device)

            go(1, zpeer)
            for j in range(1, X):
                go(2 + j, dev(z, y, (x + j) % X, c))
            go(0, partner)

        def second(self):
            ref = self.region(x, c, zn)
            recv_wait(ref, self.recv.at[1])
            for j in range(1, X):
                self.forward(ref, 2 + nx + j, dev(z, y, (x + j) % X, c))
            self.forward(ref, 2, partner)

        def third(self):
            for j in range(1, X):
                ref = self.region(self.xs(j), c, z)
                recv_wait(ref, self.recv.at[2 + j])
                self.forward(ref, 2 + 2 * nx + j, partner)
            for j in range(1, X):
                ref = self.region(self.xs(j), c, zn)
                recv_wait(ref, self.recv.at[2 + nx + j])
                self.forward(ref, 2 + 3 * nx + j, partner)

        def last(self):
            recv_wait(self.region(x, 1 - c, z), self.recv.at[0])
            recv_wait(self.region(x, 1 - c, zn), self.recv.at[2])
            for j in range(1, X):
                recv_wait(self.region(self.xs(j), 1 - c, z), self.recv.at[2 + 2 * nx + j])
                recv_wait(self.region(self.xs(j), 1 - c, zn), self.recv.at[2 + 3 * nx + j])

        def drained(self):
            for i in range(3 + 4 * nx):
                send_wait(self.own, self.sent.at[i])

    def slot(xx, cc, zz):
        return (xx * 2 + cc) * 2 + 1 - ((zz + 1) // 2) % 2

    def hidden_gather(layer, k):
        if layer == 0:
            return Gather(
                lambda xx, cc, zz: xg.at[zz % 2, :, lanes((xx * 2 + cc) * 2 * ds_, 2 * ds_)],
                h_recv.at[0], h_send.at[0], hid,
            )
        return Gather(
            lambda xx, cc, zz: xg.at[k, :, lanes(slot(xx, cc, zz) * ds_, ds_)],
            h_recv.at[k], h_send.at[k], state.at[k],
        )

    def mixed_gather(k):
        return Gather(
            lambda xx, cc, zz: mg.at[k, :, lanes(slot(xx, cc, zz) * cs, cs)],
            m_recv.at[k], m_send.at[k],
        )

    def normalise(layer, k):
        gain = ngain.at[layer]

        @pl.loop(0, T // 16)
        def _(i):
            rows = pl.ds(pl.multiple_of(i * 16, 16), 16)
            v = xg[k, rows, :].astype(jnp.float32)
            scale = lax.rsqrt(jnp.mean(v * v, axis=-1, keepdims=True) + 1e-6)
            xn[rows, :] = (v * scale * gain[...][None, :]).astype(jnp.bfloat16)

    def matmul(acc, lhs, rhs, depth, count):
        acc[...] = jnp.zeros_like(acc)

        @pl.loop(0, count)
        def _(b):
            acc[...] += jnp.dot(
                lhs[:, lanes(b * depth, depth)], rhs[b], preferred_element_type=jnp.float32
            )

    def project(layer, k):
        matmul(prod, xn, wp_buf.at[layer], D // (Z * Y), Z * Y)

        @pl.loop(0, T // HALO)
        def _(i):
            rows = pl.ds(pl.multiple_of(i * HALO, HALO), HALO)
            v, g = prod[rows, 0:cs], prod[rows, cs : 2 * cs]
            r = (v * jax.nn.sigmoid(g)).astype(jnp.bfloat16)
            glu[k, pl.ds(pl.multiple_of(i * HALO + HALO, HALO), HALO), :] = r.astype(jnp.float32)

        tail[layer, k] = glu[k, T : T + HALO, :].astype(jnp.bfloat16)

    def tail_send(layer, k):
        def go(kk, device):
            send(tail.at[layer, k], halo.at[layer, kk], t_send.at[layer, k], t_recv.at[layer, kk], device)

        @pl.when(y < Y - 1)
        def _():
            go(k, dev(z, y + 1, x, c))

        if k == 0:
            @pl.when(y == Y - 1)
            def _():
                go(1, dev(z, 0, x, c))
        else:
            @pl.when((y == Y - 1) & (zh == 0))
            def _():
                go(0, dev(Z - 1 - z, 0, x, c))

    def tail_sent(layer, k):
        if k == 0:
            send_wait(tail.at[layer, k], t_send.at[layer, k])
        else:
            @pl.when((y < Y - 1) | (zh == 0))
            def _():
                send_wait(tail.at[layer, k], t_send.at[layer, k])

    def tail_recv(layer, k):
        def arrive():
            recv_wait(halo.at[layer, k], t_recv.at[layer, k])
            glu[k, 0:HALO, :] = halo[layer, k].astype(jnp.float32)

        if k == 1:
            arrive()
        else:
            @pl.when((y > 0) | (zh > 0))
            def _():
                arrive()

            @pl.when((y == 0) & (zh == 0))
            def _():
                glu[k, 0:HALO, :] = jnp.zeros((HALO, cs), jnp.float32)

    def convolve(layer, k):
        first_lane = lax.broadcasted_iota(jnp.int32, (ROWS, 128), 1) == 0

        @pl.loop(0, T // ROWS)
        def _(i):
            base = pl.multiple_of(i * ROWS, ROWS)
            near = pos[k, pl.ds(base, ROWS), :]
            total = jnp.zeros((ROWS, 128), jnp.float32)
            square = jnp.zeros((ROWS, 128), jnp.float32)
            for t in range(cs // 128):
                at = lanes(h * cs + t * 128, 128)
                span = glu[k, pl.ds(base, ROWS + HALO), t * 128 : (t + 1) * 128]
                acc = jnp.broadcast_to(cbias[layer : layer + 1, at], (ROWS, 128))
                for phase in range(8):
                    moved = span if phase == 0 else pltpu.roll(span, ROWS + HALO - phase, 0)
                    for off in range(phase, HALO + 1, 8):
                        index = off - (HALO - (WIDTH - 1))
                        if 0 <= index < WIDTH:
                            start = off - phase
                            term = moved[start : start + ROWS] * taps[layer, index : index + 1, at]
                            back = WIDTH - 1 - index
                            acc = acc + (jnp.where(near >= back, term, 0.0) if back else term)
                conv[k, pl.ds(base, ROWS), t * 128 : (t + 1) * 128] = acc
                total = total + acc
                square = square + acc * acc
            s1 = jnp.sum(total, axis=1, keepdims=True)
            s2 = jnp.sum(square, axis=1, keepdims=True)
            stat[pl.ds(base, ROWS), :] = jnp.where(first_lane, s1, s2)

        for t in range(T // 128):
            stat_out[k, :, t * 128 : (t + 1) * 128] = stat[t * 128 : (t + 1) * 128, :].T[0:8, :]

    def others():
        for xj in range(X):
            for cj in range(2):
                for zj in range(2):
                    if xj or cj or zj:
                        xx, cc = (x + xj) % X, (c + cj) % 2
                        zz, zb = (zn, zn) if zj else (z, z)
                        back = ((x - xj + X) % X, (c + cj) % 2, zz)
                        yield (xj * 2 + cj) * 2 + zj, dev(zz, y, xx, cc), slot(*back)

    def stats_send(k):
        for i, device, _ in others():
            send(stat_out.at[k], stat_in.at[k, me], s_send.at[k, i], s_recv.at[k, i], device)

    def mix(layer, k):
        for i, _, theirs in others():
            recv_wait(stat_in.at[k, theirs], s_recv.at[k, i])
        stat_in[k, me] = stat_out[k]
        total = stat_in[k, 0]
        for i in range(1, S):
            total = total + stat_in[k, i]
        for t in range(T // 128):
            tile = total[:, t * 128 : (t + 1) * 128]
            turned = jnp.concatenate([tile] * 16, axis=0).T
            mu = turned[:, 0:1] * (1.0 / C)
            var = turned[:, 1:2] * (1.0 / C) - mu * mu
            rows = slice(t * 128, (t + 1) * 128)
            cols[0, rows, :] = jnp.broadcast_to(mu, (128, 128))
            cols[1, rows, :] = jnp.broadcast_to(lax.rsqrt(var + 1e-5), (128, 128))

        @pl.loop(0, T // ROWS)
        def _(i):
            rows = pl.ds(pl.multiple_of(i * ROWS, ROWS), ROWS)
            mu, scale = cols[0, rows, :], cols[1, rows, :]
            for t in range(cs // 128):
                at = lanes(h * cs + t * 128, 128)
                v = (conv[k, rows, t * 128 : (t + 1) * 128] - mu) * scale
                v = v * cgain[layer : layer + 1, at] + chbias[layer : layer + 1, at]
                mg[k, rows, lanes(me * cs + t * 128, 128)] = jax.nn.silu(v).astype(jnp.bfloat16)

    def stats_sent(k):
        for i, _, _ in others():
            send_wait(stat_out.at[k], s_send.at[k, i])

    def contract(layer, k):
        matmul(branch, mg.at[k], wo_buf.at[layer], C // (Z * Y), Z * Y)
        state[k] = (state[k].astype(jnp.float32) + branch[...]).astype(jnp.bfloat16)

    own0 = xg.at[ko, :, lanes((x * 2 + c) * 2 * ds_, 2 * ds_)]
    local = pltpu.make_async_copy(hid, own0, f_sem.at[0])
    local.start()
    start_part(0)
    gather0 = hidden_gather(0, 0)
    gather0.first()
    event1(0)
    event2(0)
    gather0.second()
    event3(0)
    start_part(1)
    event4(0)
    gather0.third()
    local.wait()

    for layer in range(LAYERS):
        p_next, o_now, o_next = 2 * layer + 2, 2 * layer + 1, 2 * layer + 3
        more = layer + 1 < LAYERS
        event1(o_now)
        event2(o_now)
        for k in range(2):
            gh = gather0 if layer == 0 else hidden_gather(layer, k)
            if layer or k == 0:
                gh.last()
            if layer == 0:
                if k == 0:
                    for kk in range(2):
                        state[kk] = xg[kk, :, lanes(me * ds_, ds_)]
            normalise(layer, k)
            if k == 0:
                part_ready(2 * layer)
            project(layer, k)
            tail_send(layer, k)
            if layer or k == 0:
                gh.drained()
        event3(o_now)
        if more:
            start_part(p_next)
        event4(o_now)
        for k in range(2):
            tail_recv(layer, k)
            convolve(layer, k)
            stats_send(k)
        gm = [mixed_gather(k) for k in range(2)]
        for k in range(2):
            mix(layer, k)
            stats_sent(k)
            gm[k].first()
        if more:
            event1(p_next)
        for k in range(2):
            gm[k].second()
        for k in range(2):
            gm[k].third()
        if more:
            event2(p_next)
        part_ready(o_now)
        for k in range(2):
            gm[k].last()
            contract(layer, k)
            gm[k].drained()
            if more:
                xg[k, :, lanes(me * ds_, ds_)] = state[k]
                hidden_gather(layer + 1, k).first()
        if more:
            event3(p_next)
            start_part(o_next)
            for k in range(2):
                hidden_gather(layer + 1, k).second()
            event4(p_next)
            for k in range(2):
                hidden_gather(layer + 1, k).third()

    half = final.at[:, lanes(h * ds_, ds_)]
    send(state.at[1 - ko], half, f_sem.at[1], f_sem.at[2], zpeer)
    final[:, lanes(h * ds_, ds_)] = state[ko]
    for layer in range(LAYERS):
        for k in range(2):
            tail_sent(layer, k)
    for q in range(parts):
        part_sent(q)
    send_wait(half, f_sem.at[1])
    recv_wait(final.at[:, lanes((1 - h) * ds_, ds_)], f_sem.at[2])
    done = pltpu.make_async_copy(final, out, f_sem.at[0])
    done.start()
    done.wait()


def per_device(
    sizes, hidden, doc_ids, norm_gain, w_value, w_gate, conv_taps, conv_bias, chan_gain, chan_bias, w_out
):
    SP, TP = sizes
    Z, Y = grid_of(SP)
    X = TP // 2
    T = hidden.shape[0]
    D = hidden.shape[1] * TP
    C = w_value.shape[2] * TP
    LAYERS, WIDTH = conv_taps.shape[0], conv_taps.shape[1]
    S = 4 * X
    cs, ds_ = C // S, D // S
    rp, ro = D // SP, C // SP
    bf, f32 = jnp.bfloat16, jnp.float32

    docs = lax.all_gather(doc_ids, "sp", tiled=True)
    spi = lax.axis_index("sp")
    z, y = spi // Y, spi % Y
    starts = jnp.stack([((z // 2) * 2 + k) * Y + y for k in range(2)]) * T
    where = starts[:, None] + jnp.arange(T)[None, :]
    mine = jnp.stack([lax.dynamic_slice_in_dim(docs, starts[k], T) for k in range(2)])
    before = jnp.sum((docs[None, None, :] < mine[:, :, None]).astype(jnp.int32), axis=-1)
    pos = jnp.broadcast_to((where - before)[:, :, None], (2, T, 128)).astype(jnp.int32)

    dims = (Z, Y, X, T, D, C, LAYERS, WIDTH)
    parts = 2 * LAYERS
    nx, ny = X - 1, Y - 1
    dma = pltpu.SemaphoreType.DMA
    vm = pl.BlockSpec(memory_space=pltpu.VMEM)
    hbm = pl.BlockSpec(memory_space=pl.ANY)
    return pl.pallas_call(
        functools.partial(kernel, dims),
        out_shape=jax.ShapeDtypeStruct((T, 2 * ds_), bf),
        in_specs=[hbm, vm, vm, hbm, hbm, vm, vm, vm, vm, hbm],
        out_specs=hbm,
        scratch_shapes=[
            pltpu.VMEM((LAYERS, SP, rp, 2 * cs), bf),
            pltpu.VMEM((LAYERS, SP, ro, ds_), bf),
            pltpu.VMEM((LAYERS, 3, rp, 2 * cs), bf),
            pltpu.VMEM((LAYERS, 3, ro, ds_), bf),
            pltpu.VMEM((2, T, D), bf),
            pltpu.VMEM((T, D), bf),
            pltpu.VMEM((2, T, C), bf),
            pltpu.VMEM((T, 2 * cs), f32),
            pltpu.VMEM((T, ds_), f32),
            pltpu.VMEM((2, T + HALO, cs), f32),
            pltpu.VMEM((2, T, cs), f32),
            pltpu.VMEM((2, T, ds_), bf),
            pltpu.VMEM((T, 2 * ds_), bf),
            pltpu.VMEM((LAYERS, 2, HALO, cs), bf),
            pltpu.VMEM((LAYERS, 2, HALO, cs), bf),
            pltpu.VMEM((T, 128), f32),
            pltpu.VMEM((2, 8, T), f32),
            pltpu.VMEM((2, S, 8, T), f32),
            pltpu.VMEM((2, T, 128), f32),
            dma((parts,)),
            dma((parts, 3)),
            dma((parts, 3)),
            dma((parts, Z, ny)),
            dma((parts, 7)),
            dma((parts, Z, ny)),
            dma((2, 3 + 4 * nx)),
            dma((2, 3 + 4 * nx)),
            dma((2, 3 + 4 * nx)),
            dma((2, 3 + 4 * nx)),
            dma((2, S)),
            dma((2, S)),
            dma((LAYERS, 2)),
            dma((LAYERS, 2)),
            dma((3,)),
        ],
        compiler_params=pltpu.CompilerParams(has_side_effects=True, vmem_limit_bytes=60 << 20),
        name="stack",
    )(hidden, pos, norm_gain, w_value, w_gate, conv_taps, conv_bias, chan_gain, chan_bias, w_out)


def solution(mesh):
    placed = (
        P("sp", "tp"),
        P("sp"),
        P(),
        P(None, "sp", "tp"),
        P(None, "sp", "tp"),
        P(None, None, "tp"),
        P(None, "tp"),
        P(None, "tp"),
        P(None, "tp"),
        P(None, "sp", "tp"),
    )
    sizes = (mesh.shape["sp"], mesh.shape["tp"])
    return jax.shard_map(
        functools.partial(per_device, sizes),
        mesh=mesh,
        in_specs=placed,
        out_specs=P("sp", "tp"),
        check_vma=False,
    )
```

profile of v0, /device:TPU:0, one launch (start us, length us, event | category | flops | bytes accessed | tf_op | source)
XLA Modules:
  0.0 376.4 jit_solution(4015444992624510027)
XLA Ops:
  0.0 0.1 add_multiply_fusion
  0.1 0.7 fusion.1
  4.8 0.7 reshape.42
  5.4 27.8 %all-gather = s32[8,1,384]{2,1,0:T(1,128)S(1)} all-gather(s32[1,1,384]{2,1,0:T(1,128)S(1)} %reshape.42), channel_id=1, replica_groups=mesh['sp'=8,'tp'=4] {'sp'}, dimensions={0}, use_global_device_ids=true | all-gather | bytes 13824 | tf_op jit(solution)/shard_map/all_gather | solution.py:533
  33.3 0.1 fusion
  33.4 1.1 convert_reduce_fusion
  34.5 0.1 add_subtract_fusion
  34.5 0.9 broadcast_in_dim.2.pos
  35.5 338.8 %stack.25 = bf16[384,1024]{1,0:T(8,128)(2,1)} custom-call(bf16[384,1024]{1,0:T(8,128)(2,1)} %hid.1, s32[2,384,128]{2,1,0:T(8,128)} %broadcast_in_dim.2.pos, f32[3,4096]{1,0:T(4,128)} %ngain.1, bf16[3,512,512]{2,1,0:T(8,128)(2,1)} %wv.1, bf16[3,512,512]{2,1,0:T(8,128)(2,1)} %wg.1, f32[3,31,512]{2,1,0:T(8,128)} %taps.1, f32[3,512]{1,0:T(4,128)} %cbias.1, ...), custom_call_target="tpu_custom_call" | custom-call | tf_op jit(solution)/shard_map/stack/pallas_call | solution.py:548
  374.3 2.1 copy.12
  (3 shorter events, 0.0 us)
where the time goes:
time: 377 us; the launch traced here: 376 us
  Pallas kernels  339 us (90%)
  blocking collectives  27.8 us (7%)
  local copies, waits for them, and re-layouts  4.42 us (1%)
  between operations  4.03 us (1%)
    pallas_call x1, Pallas kernels, per_device(): pl.pallas_call(functools.partial(kernel, dims), out_shape=jax.ShapeDtypeS...  339 us
    all_gather x1, blocking collectives, per_device(): docs = lax.all_gather(doc_ids, 'sp', tiled=True)  27.8 us

commit v1 on v0

--- a/solution.py
+++ b/solution.py
@@ -21,7 +21,7 @@
 def kernel(
     dims,
     hid,
-    pos,
+    docs,
     ngain,
     wv,
     wg,
@@ -50,6 +50,8 @@
     stat_out,
     stat_in,
     cols,
+    pos,
+    doc_halo,
     loc_sem,
     z_recv,
     r_recv,
@@ -65,6 +67,7 @@
     t_recv,
     t_send,
     f_sem,
+    d_sem,
 ):
     Z, Y, X, T, D, C, LAYERS, WIDTH = dims
     S = 4 * X
@@ -158,6 +161,7 @@
         recv_wait(block(q, zn * Y + y), z_recv.at[q, 0])
         y_spread(q, zn)
 
+    def relay1(q):
         @pl.when(inner == 1)
         def _():
             recv_wait(relay(q, 0), r_recv.at[q, 0])
@@ -239,6 +243,8 @@
                 ref = self.region(self.xs(j), c, z)
                 recv_wait(ref, self.recv.at[2 + j])
                 self.forward(ref, 2 + 2 * nx + j, partner)
+
+        def fourth(self):
             for j in range(1, X):
                 ref = self.region(self.xs(j), c, zn)
                 recv_wait(ref, self.recv.at[2 + nx + j])
@@ -276,14 +282,21 @@
         )
 
     def normalise(layer, k):
-        gain = ngain.at[layer]
-
-        @pl.loop(0, T // 16)
+        @pl.loop(0, T // 16, unroll=2)
         def _(i):
             rows = pl.ds(pl.multiple_of(i * 16, 16), 16)
             v = xg[k, rows, :].astype(jnp.float32)
             scale = lax.rsqrt(jnp.mean(v * v, axis=-1, keepdims=True) + 1e-6)
-            xn[rows, :] = (v * scale * gain[...][None, :]).astype(jnp.bfloat16)
+            cols[0, rows, :] = jnp.broadcast_to(scale, (16, 128))
+
+        @pl.loop(0, T // 16)
+        def _(i):
+            rows = pl.ds(pl.multiple_of(i * 16, 16), 16)
+            scale = cols[0, rows, :]
+            for t in range(D // 128):
+                at = slice(t * 128, (t + 1) * 128)
+                v = xg[k, rows, at].astype(jnp.float32) * scale * ngain[layer : layer + 1, at]
+                xn[rows, at] = v.astype(jnp.bfloat16)
 
     def matmul(acc, lhs, rhs, depth, count):
         acc[...] = jnp.zeros_like(acc)
@@ -427,79 +440,142 @@
         matmul(branch, mg.at[k], wo_buf.at[layer], C // (Z * Y), Z * Y)
         state[k] = (state[k].astype(jnp.float32) + branch[...]).astype(jnp.bfloat16)
 
+    def docs_start():
+        tail_docs = docs.at[pl.ds(T - HALO, HALO)]
+
+        @pl.when(y < Y - 1)
+        def _():
+            send(tail_docs, doc_halo, d_sem.at[0], d_sem.at[1], dev(z, y + 1, x, c))
+
+        @pl.when((y == Y - 1) & (z < Z - 1))
+        def _():
+            send(tail_docs, doc_halo, d_sem.at[0], d_sem.at[1], dev(z + 1, 0, x, c))
+
+    def docs_done():
+        @pl.when((y > 0) | (z > 0))
+        def _():
+            recv_wait(doc_halo, d_sem.at[1])
+
+        @pl.when((y == 0) & (z == 0))
+        def _():
+            doc_halo[...] = jnp.full((HALO, 128), -1, jnp.int32)
+
+        def count(base, span):
+            here = span[HALO:]
+            total = jnp.zeros((ROWS, 128), jnp.int32)
+            for phase in range(8):
+                moved = span if phase == 0 else pltpu.roll(span, ROWS + HALO - phase, 0)
+                for off in range(phase, HALO, 8):
+                    if off >= HALO - (WIDTH - 1):
+                        start = off - phase
+                        same = moved[start : start + ROWS] == here
+                        total = total + jnp.where(same, 1, 0)
+            pos[ko, pl.ds(base, ROWS), :] = total
+
+        count(0, jnp.concatenate([doc_halo[...], docs[0:ROWS, :]], axis=0))
+
+        @pl.loop(1, T // ROWS)
+        def _(i):
+            base = pl.multiple_of(i * ROWS, ROWS)
+            count(base, docs[pl.ds(pl.multiple_of(base - HALO, HALO), ROWS + HALO), :])
+
+        send(pos.at[ko], pos.at[ko], d_sem.at[2], d_sem.at[3], zpeer)
+
+    def docs_sent():
+        @pl.when((y < Y - 1) | (z < Z - 1))
+        def _():
+            send_wait(doc_halo, d_sem.at[0])
+
+        send_wait(pos.at[ko], d_sem.at[2])
+
     own0 = xg.at[ko, :, lanes((x * 2 + c) * 2 * ds_, 2 * ds_)]
     local = pltpu.make_async_copy(hid, own0, f_sem.at[0])
     local.start()
+    docs_start()
     start_part(0)
-    gather0 = hidden_gather(0, 0)
-    gather0.first()
+    gh = [hidden_gather(0, 0)]
+    gh[0].first()
+    docs_done()
     event1(0)
+    relay1(0)
     event2(0)
-    gather0.second()
+    start_part(1)
+    gh[0].second()
     event3(0)
-    start_part(1)
+    gh[0].third()
+    local.wait()
     event4(0)
-    gather0.third()
-    local.wait()
 
     for layer in range(LAYERS):
-        p_next, o_now, o_next = 2 * layer + 2, 2 * layer + 1, 2 * layer + 3
+        p_now, o_now, p_next = 2 * layer, 2 * layer + 1, 2 * layer + 2
         more = layer + 1 < LAYERS
+        if layer:
+            event3(p_now)
+            gh[0].second()
+            gh[0].third()
+            start_part(o_now)
+            event4(p_now)
+            gh[1].second()
+            gh[1].third()
         event1(o_now)
+        relay1(o_now)
         event2(o_now)
         for k in range(2):
-            gh = gather0 if layer == 0 else hidden_gather(layer, k)
-            if layer or k == 0:
-                gh.last()
-            if layer == 0:
-                if k == 0:
-                    for kk in range(2):
-                        state[kk] = xg[kk, :, lanes(me * ds_, ds_)]
+            if k < len(gh):
+                gh[k].fourth()
+                gh[k].last()
+            if layer == 0 and k == 0:
+                for kk in range(2):
+                    state[kk] = xg[kk, :, lanes(me * ds_, ds_)]
             normalise(layer, k)
             if k == 0:
-                part_ready(2 * layer)
+                part_ready(p_now)
             project(layer, k)
             tail_send(layer, k)
-            if layer or k == 0:
-                gh.drained()
-        event3(o_now)
-        if more:
-            start_part(p_next)
+            if k < len(gh):
+                gh[k].drained()
+            if k == 0:
+                event3(o_now)
+                if more:
+                    start_part(p_next)
         event4(o_now)
+        if layer == 0:
+            recv_wait(pos.at[1 - ko], d_sem.at[3])
         for k in range(2):
             tail_recv(layer, k)
+            if layer:
+                stats_sent(k)
             convolve(layer, k)
             stats_send(k)
+        if more:
+            event1(p_next)
         gm = [mixed_gather(k) for k in range(2)]
         for k in range(2):
             mix(layer, k)
-            stats_sent(k)
             gm[k].first()
         if more:
-            event1(p_next)
+            relay1(p_next)
         for k in range(2):
             gm[k].second()
-        for k in range(2):
             gm[k].third()
         if more:
             event2(p_next)
-        part_ready(o_now)
         for k in range(2):
+            gm[k].fourth()
             gm[k].last()
+            if k == 0:
+                part_ready(o_now)
             contract(layer, k)
             gm[k].drained()
             if more:
                 xg[k, :, lanes(me * ds_, ds_)] = state[k]
-                hidden_gather(layer + 1, k).first()
-        if more:
-            event3(p_next)
-            start_part(o_next)
-            for k in range(2):
-                hidden_gather(layer + 1, k).second()
-            event4(p_next)
-            for k in range(2):
-                hidden_gather(layer + 1, k).third()
-
+                if k == 0:
+                    gh = [hidden_gather(layer + 1, kk) for kk in range(2)]
+                gh[k].first()
+
+    for k in range(2):
+        stats_sent(k)
+    docs_sent()
     half = final.at[:, lanes(h * ds_, ds_)]
     send(state.at[1 - ko], half, f_sem.at[1], f_sem.at[2], zpeer)
     final[:, lanes(h * ds_, ds_)] = state[ko]
@@ -530,14 +606,7 @@
     rp, ro = D // SP, C // SP
     bf, f32 = jnp.bfloat16, jnp.float32
 
-    docs = lax.all_gather(doc_ids, "sp", tiled=True)
-    spi = lax.axis_index("sp")
-    z, y = spi // Y, spi % Y
-    starts = jnp.stack([((z // 2) * 2 + k) * Y + y for k in range(2)]) * T
-    where = starts[:, None] + jnp.arange(T)[None, :]
-    mine = jnp.stack([lax.dynamic_slice_in_dim(docs, starts[k], T) for k in range(2)])
-    before = jnp.sum((docs[None, None, :] < mine[:, :, None]).astype(jnp.int32), axis=-1)
-    pos = jnp.broadcast_to((where - before)[:, :, None], (2, T, 128)).astype(jnp.int32)
+    docs = jnp.broadcast_to(doc_ids[:, None], (T, 128))
 
     dims = (Z, Y, X, T, D, C, LAYERS, WIDTH)
     parts = 2 * LAYERS
@@ -570,6 +639,8 @@
             pltpu.VMEM((2, 8, T), f32),
             pltpu.VMEM((2, S, 8, T), f32),
             pltpu.VMEM((2, T, 128), f32),
+            pltpu.VMEM((2, T, 128), jnp.int32),
+            pltpu.VMEM((HALO, 128), jnp.int32),
             dma((parts,)),
             dma((parts, 3)),
             dma((parts, 3)),
@@ -585,10 +656,11 @@
             dma((LAYERS, 2)),
             dma((LAYERS, 2)),
             dma((3,)),
+            dma((4,)),
         ],
         compiler_params=pltpu.CompilerParams(has_side_effects=True, vmem_limit_bytes=60 << 20),
         name="stack",
-    )(hidden, pos, norm_gain, w_value, w_gate, conv_taps, conv_bias, chan_gain, chan_bias, w_out)
+    )(hidden, docs, norm_gain, w_value, w_gate, conv_taps, conv_bias, chan_gain, chan_bias, w_out)
 
 
 def solution(mesh):

time: 377 us -> 336 us (0.89)
  blocking collectives: 27.8 us -> 0 us
  Pallas kernels: 339 us -> 330 us
  between operations: 4.03 us -> 0.01 us
    all_gather x1 -> x0, blocking collectives: 27.8 us -> none  [per_device(): docs = lax.all_gather(doc_ids, 'sp', tiled=True)]
    pallas_call x1, Pallas kernels: 339 us -> 330 us  [per_device(): pl.pallas_call(functools.partial(kernel, dims), out_shape=jax.ShapeDtypeS...]
where the time goes in v1:
time: 336 us; the launch traced here: 334 us
  Pallas kernels  330 us (98%)
  local copies, waits for them, and re-layouts  3.54 us (1%)
    pallas_call x1, Pallas kernels, per_device(): pl.pallas_call(functools.partial(kernel, dims), out_shape=jax.ShapeDtypeS...  330 us

profile of v1, /device:TPU:0, one launch (start us, length us, event | category | flops | bytes accessed | tf_op | source)
XLA Modules:
  0.0 333.7 jit_solution(17762759953542620100)
XLA Ops:
  0.0 1.5 broadcast_in_dim.2.docs
  1.5 330.2 %stack.1 = bf16[384,1024]{1,0:T(8,128)(2,1)} custom-call(bf16[384,1024]{1,0:T(8,128)(2,1)} %hid.1, s32[384,128]{1,0:T(8,128)} %broadcast_in_dim.2.docs, f32[3,4096]{1,0:T(4,128)} %ngain.1, bf16[3,512,512]{2,1,0:T(8,128)(2,1)} %wv.1, bf16[3,512,512]{2,1,0:T(8,128)(2,1)} %wg.1, f32[3,31,512]{2,1,0:T(8,128)} %taps.1, f32[3,512]{1,0:T(4,128)} %cbias.1, ...), custom_call_target="tpu_custom_call" | custom-call | tf_op jit(solution)/shard_map/stack/pallas_call | solution.py:617
  331.7 2.1 copy.12

commit v2 on v1

--- a/solution.py
+++ b/solution.py
@@ -33,8 +33,8 @@
     out,
     wp_buf,
     wo_buf,
-    rp_buf,
-    ro_buf,
+    stage_p,
+    stage_o,
     xg,
     xn,
     mg,
@@ -49,12 +49,15 @@
     stat,
     stat_out,
     stat_in,
+    stat_row,
+    tail_relay,
     cols,
     pos,
     doc_halo,
     loc_sem,
+    g_recv,
+    g_send,
     z_recv,
-    r_recv,
     y_recv,
     z_send,
     y_send,
@@ -64,6 +67,10 @@
     m_send,
     s_recv,
     s_send,
+    r_recv,
+    r_send,
+    k_recv,
+    k_send,
     t_recv,
     t_send,
     f_sem,
@@ -90,7 +97,6 @@
 
     partner = dev(z, y, x, 1 - c)
     zpeer = dev(zn, y, x, c)
-    mid = dev(Z - 1 - z, y, x, c)
 
     def send(src, dst, ssem, rsem, device):
         pltpu.make_async_remote_copy(
@@ -116,21 +122,59 @@
     def block(q, b):
         return (wo_buf if q % 2 else wp_buf).at[q // 2, b]
 
-    def relay(q, i):
-        return (ro_buf if q % 2 else rp_buf).at[q // 2, i]
-
-    def own_pieces(q, half, dst):
+    def own_pieces(q, half, dst, staged=False):
         l = q // 2
         if q % 2:
-            return [(wo.at[l, :, lanes(half * ds_, ds_)], dst)]
+            src = stage_o if staged else wo
+            return [(src.at[l, :, lanes(half * ds_, ds_)], dst)]
+        low, high = dst.at[:, pl.ds(0, cs)], dst.at[:, pl.ds(cs, cs)]
+        if staged:
+            return [
+                (stage_p.at[l, :, lanes(half * cs, cs)], low),
+                (stage_p.at[l, :, lanes((half + 2) * cs, cs)], high),
+            ]
         return [
-            (wv.at[l, :, lanes(half * cs, cs)], dst.at[:, pl.ds(0, cs)]),
-            (wg.at[l, :, lanes(half * cs, cs)], dst.at[:, pl.ds(cs, cs)]),
+            (wv.at[l, :, lanes(half * cs, cs)], low),
+            (wg.at[l, :, lanes(half * cs, cs)], high),
         ]
 
-    def own_send(q, half, dst, ssem, rsem, device):
-        for src, part in own_pieces(q, half, dst):
+    def own_send(q, half, dst, ssem, rsem, device, staged=False):
+        for src, part in own_pieces(q, half, dst, staged):
             send(src, part, ssem, rsem, device)
+
+    def hand_over(q):
+        l = q // 2
+        if q % 2:
+            moves = [(wo.at[l], stage_o.at[l])]
+        else:
+            moves = [
+                (wv.at[l], stage_p.at[l, :, pl.ds(0, 2 * cs)]),
+                (wg.at[l], stage_p.at[l, :, pl.ds(2 * cs, 2 * cs)]),
+            ]
+        for src, dst in moves:
+            send(src, dst, g_send.at[q], g_recv.at[q], partner)
+
+    def staged_ref(q):
+        return (stage_o if q % 2 else stage_p).at[q // 2]
+
+    def z_sends(q):
+        mine = block(q, z * Y + y)
+        moves = [
+            (1 - h, z_recv.at[q, 0], zn),
+            (h, z_recv.at[q, 1 + h], Z - 1 - z),
+            (1 - h, z_recv.at[q, 1 + h], Z - 1 - zn),
+        ]
+        for i, (half, rsem, zz) in enumerate(moves):
+            for cc in (1, 0):
+                if i == 0 and cc == 0:
+                    recv_wait(staged_ref(q), g_recv.at[q])
+                own_send(q, half, mine, z_send.at[q, cc, i], rsem, dev(zz, y, x, cc), cc == 0)
+
+    def z_start(*qs, kind=None):
+        @pl.when((c == 1) if kind is None else (c == 1) & (inner == kind))
+        def _():
+            for q in qs:
+                z_sends(q)
 
     def y_spread(q, zb):
         b = zb * Y + y
@@ -140,17 +184,6 @@
 
     def start_part(q):
         mine = block(q, z * Y + y)
-        own_send(q, 1 - h, mine, z_send.at[q, 0], z_recv.at[q, 0], zpeer)
-
-        @pl.when(inner == 0)
-        def _():
-            own_send(q, h, relay(q, 1), z_send.at[q, 1], r_recv.at[q, 1], zpeer)
-
-        @pl.when(inner == 1)
-        def _():
-            own_send(q, 1 - h, relay(q, 0), z_send.at[q, 1], r_recv.at[q, 0], mid)
-            own_send(q, h, mine, z_send.at[q, 2], z_recv.at[q, 1], mid)
-
         for j in range(1, Y):
             own_send(q, h, mine, y_send.at[q, z, j - 1], y_recv.at[q, z, j - 1],
                      dev(z, (y + j) % Y, x, c))
@@ -161,31 +194,12 @@
         recv_wait(block(q, zn * Y + y), z_recv.at[q, 0])
         y_spread(q, zn)
 
-    def relay1(q):
-        @pl.when(inner == 1)
-        def _():
-            recv_wait(relay(q, 0), r_recv.at[q, 0])
-            send(relay(q, 0), block(q, (Z - 1 - z) * Y + y), z_send.at[q, 3], z_recv.at[q, 1], zpeer)
-
     def event2(q):
-        @pl.when(inner == 1)
-        def _():
-            recv_wait(relay(q, 1), r_recv.at[q, 1])
-            send(relay(q, 1), relay(q, 2), z_send.at[q, 4], r_recv.at[q, 2], mid)
-            near = block(q, zn * Y + y)
-            send(near, near, z_send.at[q, 5], z_recv.at[q, 2], mid)
-
         zb = Z - 1 - zin
         recv_wait(block(q, zb * Y + y), z_recv.at[q, 1])
         y_spread(q, zb)
 
     def event3(q):
-        @pl.when(inner == 1)
-        def _():
-            recv_wait(relay(q, 2), r_recv.at[q, 2])
-            send(relay(q, 2), block(q, (Z - 1 - zn) * Y + y), z_send.at[q, 6], z_recv.at[q, 2], zpeer)
-
-    def event4(q):
         zb = Z - 1 - zout
         recv_wait(block(q, zb * Y + y), z_recv.at[q, 2])
         y_spread(q, zb)
@@ -202,13 +216,16 @@
         for zb in range(Z):
             for j in range(1, Y):
                 send_wait(ref, y_send.at[q, zb, j - 1])
-        send_wait(ref, z_send.at[q, 0])
-        send_wait(ref, z_send.at[q, 1])
-
-        @pl.when(inner == 1)
-        def _():
-            for i in range(2, 7):
-                send_wait(ref, z_send.at[q, i])
+
+        @pl.when(c == 1)
+        def _():
+            for cc in range(2):
+                for i in range(3):
+                    send_wait(ref, z_send.at[q, cc, i])
+
+        @pl.when(c == 0)
+        def _():
+            send_wait(staged_ref(q), g_send.at[q])
 
     class Gather:
         def __init__(self, region, recv, sent, source=None):
@@ -226,10 +243,20 @@
             def go(i, device):
                 send(self.source, self.own, self.sent.at[i], self.recv.at[i], device)
 
-            go(1, zpeer)
             for j in range(1, X):
                 go(2 + j, dev(z, y, (x + j) % X, c))
             go(0, partner)
+
+            @pl.when(c == 0)
+            def _():
+                go(1, zpeer)
+
+        def across(self):
+            @pl.when(c == 0)
+            def _():
+                ref = self.region(x, 1, z)
+                recv_wait(ref, self.recv.at[0])
+                send(ref, ref, self.sent.at[3 + 4 * nx], self.recv.at[1], dev(zn, y, x, 1))
 
         def second(self):
             ref = self.region(x, c, zn)
@@ -251,15 +278,23 @@
                 self.forward(ref, 2 + 3 * nx + j, partner)
 
         def last(self):
-            recv_wait(self.region(x, 1 - c, z), self.recv.at[0])
+            @pl.when(c == 1)
+            def _():
+                recv_wait(self.region(x, 0, z), self.recv.at[0])
+
             recv_wait(self.region(x, 1 - c, zn), self.recv.at[2])
             for j in range(1, X):
                 recv_wait(self.region(self.xs(j), 1 - c, z), self.recv.at[2 + 2 * nx + j])
                 recv_wait(self.region(self.xs(j), 1 - c, zn), self.recv.at[2 + 3 * nx + j])
 
         def drained(self):
-            for i in range(3 + 4 * nx):
+            for i in [0] + list(range(2, 3 + 4 * nx)):
                 send_wait(self.own, self.sent.at[i])
+
+            @pl.when(c == 0)
+            def _():
+                send_wait(self.own, self.sent.at[1])
+                send_wait(self.own, self.sent.at[3 + 4 * nx])
 
     def slot(xx, cc, zz):
         return (xx * 2 + cc) * 2 + 1 - ((zz + 1) // 2) % 2
@@ -317,7 +352,15 @@
             r = (v * jax.nn.sigmoid(g)).astype(jnp.bfloat16)
             glu[k, pl.ds(pl.multiple_of(i * HALO + HALO, HALO), HALO), :] = r.astype(jnp.float32)
 
-        tail[layer, k] = glu[k, T : T + HALO, :].astype(jnp.bfloat16)
+    def project_tail(layer, k):
+        rows = slice(T - HALO, T)
+
+        def step(b, acc):
+            lhs = xn[rows, lanes(b * (D // (Z * Y)), D // (Z * Y))]
+            return acc + jnp.dot(lhs, wp_buf[layer, b], preferred_element_type=jnp.float32)
+
+        both = lax.fori_loop(0, Z * Y, step, jnp.zeros((HALO, 2 * cs), jnp.float32))
+        tail[layer, k] = (both[:, 0:cs] * jax.nn.sigmoid(both[:, cs:])).astype(jnp.bfloat16)
 
     def tail_send(layer, k):
         def go(kk, device):
@@ -332,9 +375,16 @@
             def _():
                 go(1, dev(z, 0, x, c))
         else:
-            @pl.when((y == Y - 1) & (zh == 0))
-            def _():
-                go(0, dev(Z - 1 - z, 0, x, c))
+            @pl.when((y == Y - 1) & (zh == 0) & (c == 0))
+            def _():
+                go(0, dev(Z - 1 - z, 0, x, 0))
+                recv_wait(tail_relay.at[layer], k_recv.at[layer])
+                send(tail_relay.at[layer], halo.at[layer, 0], k_send.at[layer], t_recv.at[layer, 0],
+                     dev(Z - 1 - z, 0, x, 1))
+
+            @pl.when((y == Y - 1) & (zh == 0) & (c == 1))
+            def _():
+                send(tail.at[layer, k], tail_relay.at[layer], t_send.at[layer, k], k_recv.at[layer], partner)
 
     def tail_sent(layer, k):
         if k == 0:
@@ -344,6 +394,10 @@
             def _():
                 send_wait(tail.at[layer, k], t_send.at[layer, k])
 
+            @pl.when((y == Y - 1) & (zh == 0) & (c == 0))
+            def _():
+                send_wait(tail_relay.at[layer], k_send.at[layer])
+
     def tail_recv(layer, k):
         def arrive():
             recv_wait(halo.at[layer, k], t_recv.at[layer, k])
@@ -360,59 +414,69 @@
             def _():
                 glu[k, 0:HALO, :] = jnp.zeros((HALO, cs), jnp.float32)
 
+    def convolve_tile(layer, k, base):
+        first_lane = lax.broadcasted_iota(jnp.int32, (ROWS, 128), 1) == 0
+        near = pos[k, pl.ds(base, ROWS), :]
+        total = jnp.zeros((ROWS, 128), jnp.float32)
+        square = jnp.zeros((ROWS, 128), jnp.float32)
+        for t in range(cs // 128):
+            at = lanes(h * cs + t * 128, 128)
+            span = glu[k, pl.ds(base, ROWS + HALO), t * 128 : (t + 1) * 128]
+            acc = jnp.broadcast_to(cbias[layer : layer + 1, at], (ROWS, 128))
+            for phase in range(8):
+                moved = span if phase == 0 else pltpu.roll(span, ROWS + HALO - phase, 0)
+                for off in range(phase, HALO + 1, 8):
+                    index = off - (HALO - (WIDTH - 1))
+                    if 0 <= index < WIDTH:
+                        start = off - phase
+                        term = moved[start : start + ROWS] * taps[layer, index : index + 1, at]
+                        back = WIDTH - 1 - index
+                        acc = acc + (jnp.where(near >= back, term, 0.0) if back else term)
+            conv[k, pl.ds(base, ROWS), t * 128 : (t + 1) * 128] = acc
+            total = total + acc
+            square = square + acc * acc
+        s1 = jnp.sum(total, axis=1, keepdims=True)
+        s2 = jnp.sum(square, axis=1, keepdims=True)
+        stat[k, pl.ds(base, ROWS), :] = jnp.where(first_lane, s1, s2)
+
     def convolve(layer, k):
-        first_lane = lax.broadcasted_iota(jnp.int32, (ROWS, 128), 1) == 0
-
-        @pl.loop(0, T // ROWS)
+        @pl.loop(1, T // ROWS)
         def _(i):
-            base = pl.multiple_of(i * ROWS, ROWS)
-            near = pos[k, pl.ds(base, ROWS), :]
-            total = jnp.zeros((ROWS, 128), jnp.float32)
-            square = jnp.zeros((ROWS, 128), jnp.float32)
-            for t in range(cs // 128):
-                at = lanes(h * cs + t * 128, 128)
-                span = glu[k, pl.ds(base, ROWS + HALO), t * 128 : (t + 1) * 128]
-                acc = jnp.broadcast_to(cbias[layer : layer + 1, at], (ROWS, 128))
-                for phase in range(8):
-                    moved = span if phase == 0 else pltpu.roll(span, ROWS + HALO - phase, 0)
-                    for off in range(phase, HALO + 1, 8):
-                        index = off - (HALO - (WIDTH - 1))
-                        if 0 <= index < WIDTH:
-                            start = off - phase
-                            term = moved[start : start + ROWS] * taps[layer, index : index + 1, at]
-                            back = WIDTH - 1 - index
-                            acc = acc + (jnp.where(near >= back, term, 0.0) if back else term)
-                conv[k, pl.ds(base, ROWS), t * 128 : (t + 1) * 128] = acc
-                total = total + acc
-                square = square + acc * acc
-            s1 = jnp.sum(total, axis=1, keepdims=True)
-            s2 = jnp.sum(square, axis=1, keepdims=True)
-            stat[pl.ds(base, ROWS), :] = jnp.where(first_lane, s1, s2)
-
+            convolve_tile(layer, k, pl.multiple_of(i * ROWS, ROWS))
+
+    def convolve_first(layer, k):
+        convolve_tile(layer, k, 0)
         for t in range(T // 128):
-            stat_out[k, :, t * 128 : (t + 1) * 128] = stat[t * 128 : (t + 1) * 128, :].T[0:8, :]
+            stat_out[k, :, t * 128 : (t + 1) * 128] = stat[k, t * 128 : (t + 1) * 128, :].T[0:8, :]
 
     def others():
         for xj in range(X):
             for cj in range(2):
-                for zj in range(2):
-                    if xj or cj or zj:
-                        xx, cc = (x + xj) % X, (c + cj) % 2
-                        zz, zb = (zn, zn) if zj else (z, z)
-                        back = ((x - xj + X) % X, (c + cj) % 2, zz)
-                        yield (xj * 2 + cj) * 2 + zj, dev(zz, y, xx, cc), slot(*back)
+                if xj or cj:
+                    device = dev(z, y, (x + xj) % X, (c + cj) % 2)
+                    yield xj * 2 + cj, device, (x - xj + X) % X * 2 + (c + cj) % 2
 
     def stats_send(k):
         for i, device, _ in others():
-            send(stat_out.at[k], stat_in.at[k, me], s_send.at[k, i], s_recv.at[k, i], device)
-
-    def mix(layer, k):
+            send(stat_out.at[k], stat_in.at[k, x * 2 + c], s_send.at[k, i], s_recv.at[k, i], device)
+
+    def row_sum(k):
         for i, _, theirs in others():
             recv_wait(stat_in.at[k, theirs], s_recv.at[k, i])
-        stat_in[k, me] = stat_out[k]
+        stat_in[k, x * 2 + c] = stat_out[k]
         total = stat_in[k, 0]
-        for i in range(1, S):
+        for i in range(1, 2 * X):
             total = total + stat_in[k, i]
+        stat_row[k, h] = total
+
+        @pl.when(c == 0)
+        def _():
+            for cc in range(2):
+                send(stat_row.at[k, h], stat_row.at[k, h], r_send.at[k, cc], r_recv.at[k], dev(zn, y, x, cc))
+
+    def mix(layer, k):
+        recv_wait(stat_row.at[k, 1 - h], r_recv.at[k])
+        total = stat_row[k, 0] + stat_row[k, 1]
         for t in range(T // 128):
             tile = total[:, t * 128 : (t + 1) * 128]
             turned = jnp.concatenate([tile] * 16, axis=0).T
@@ -435,6 +499,11 @@
     def stats_sent(k):
         for i, _, _ in others():
             send_wait(stat_out.at[k], s_send.at[k, i])
+
+        @pl.when(c == 0)
+        def _():
+            for cc in range(2):
+                send_wait(stat_row.at[k, h], r_send.at[k, cc])
 
     def contract(layer, k):
         matmul(branch, mg.at[k], wo_buf.at[layer], C // (Z * Y), Z * Y)
@@ -479,47 +548,76 @@
             base = pl.multiple_of(i * ROWS, ROWS)
             count(base, docs[pl.ds(pl.multiple_of(base - HALO, HALO), ROWS + HALO), :])
 
-        send(pos.at[ko], pos.at[ko], d_sem.at[2], d_sem.at[3], zpeer)
+        @pl.when(c == 0)
+        def _():
+            send(pos.at[ko], pos.at[ko], d_sem.at[2], d_sem.at[3], dev(zn, y, x, 0))
+            send(pos.at[ko], pos.at[ko], d_sem.at[4], d_sem.at[3], dev(zn, y, x, 1))
 
     def docs_sent():
         @pl.when((y < Y - 1) | (z < Z - 1))
         def _():
             send_wait(doc_halo, d_sem.at[0])
 
-        send_wait(pos.at[ko], d_sem.at[2])
+        @pl.when(c == 0)
+        def _():
+            send_wait(pos.at[ko], d_sem.at[2])
+            send_wait(pos.at[ko], d_sem.at[4])
 
     own0 = xg.at[ko, :, lanes((x * 2 + c) * 2 * ds_, 2 * ds_)]
     local = pltpu.make_async_copy(hid, own0, f_sem.at[0])
     local.start()
     docs_start()
+
+    @pl.when(c == 0)
+    def _():
+        for q in range(parts):
+            hand_over(q)
+
     start_part(0)
+
+    z_start(0)
+
     gh = [hidden_gather(0, 0)]
     gh[0].first()
+    gh[0].across()
     docs_done()
     event1(0)
-    relay1(0)
     event2(0)
+    gh[0].third()
+    gh[0].second()
+    local.wait()
+    z_start(1, 2, kind=0)
+    event3(0)
+    z_start(1, 2, kind=1)
     start_part(1)
-    gh[0].second()
-    event3(0)
-    gh[0].third()
-    local.wait()
-    event4(0)
-
+
+    gm = None
     for layer in range(LAYERS):
         p_now, o_now, p_next = 2 * layer, 2 * layer + 1, 2 * layer + 2
         more = layer + 1 < LAYERS
+
+        def mixed_out(k):
+            gm[k].fourth()
+            gm[k].last()
+            if k == 0:
+                part_ready(o_now)
+            contract(layer, k)
+            if more:
+                xg[k, :, lanes(me * ds_, ds_)] = state[k]
+                gather = hidden_gather(layer + 1, k)
+                gather.first()
+                gather.across()
+                return gather
+
         if layer:
-            event3(p_now)
             gh[0].second()
             gh[0].third()
+            event2(p_now)
+            event3(p_now)
             start_part(o_now)
-            event4(p_now)
+            gh[1].third()
             gh[1].second()
-            gh[1].third()
-        event1(o_now)
-        relay1(o_now)
-        event2(o_now)
+            z_start(*([o_now, p_next] if more else [o_now]))
         for k in range(2):
             if k < len(gh):
                 gh[k].fourth()
@@ -530,50 +628,48 @@
             normalise(layer, k)
             if k == 0:
                 part_ready(p_now)
+            project_tail(layer, k)
+            tail_send(layer, k)
             project(layer, k)
-            tail_send(layer, k)
             if k < len(gh):
                 gh[k].drained()
             if k == 0:
-                event3(o_now)
-                if more:
-                    start_part(p_next)
-        event4(o_now)
-        if layer == 0:
-            recv_wait(pos.at[1 - ko], d_sem.at[3])
+                if layer == 0:
+                    recv_wait(pos.at[1 - ko], d_sem.at[3])
+                else:
+                    stats_sent(0)
+                    stats_sent(1)
+            convolve(layer, k)
+            if k == 0:
+                event1(o_now)
+                event2(o_now)
         for k in range(2):
             tail_recv(layer, k)
+            convolve_first(layer, k)
             if layer:
-                stats_sent(k)
-            convolve(layer, k)
+                gm[k].drained()
             stats_send(k)
+        event3(o_now)
         if more:
-            event1(p_next)
+            start_part(p_next)
+        for k in range(2):
+            row_sum(k)
         gm = [mixed_gather(k) for k in range(2)]
         for k in range(2):
             mix(layer, k)
             gm[k].first()
+            gm[k].across()
         if more:
-            relay1(p_next)
-        for k in range(2):
-            gm[k].second()
-            gm[k].third()
-        if more:
-            event2(p_next)
-        for k in range(2):
-            gm[k].fourth()
-            gm[k].last()
-            if k == 0:
-                part_ready(o_now)
-            contract(layer, k)
-            gm[k].drained()
-            if more:
-                xg[k, :, lanes(me * ds_, ds_)] = state[k]
-                if k == 0:
-                    gh = [hidden_gather(layer + 1, kk) for kk in range(2)]
-                gh[k].first()
+            event1(p_next)
+        gm[0].third()
+        gm[0].second()
+        gm[1].third()
+        gm[1].second()
+        first = mixed_out(0)
+        gh = [first, mixed_out(1)]
 
     for k in range(2):
+        gm[k].drained()
         stats_sent(k)
     docs_sent()
     half = final.at[:, lanes(h * ds_, ds_)]
@@ -622,8 +718,8 @@
         scratch_shapes=[
             pltpu.VMEM((LAYERS, SP, rp, 2 * cs), bf),
             pltpu.VMEM((LAYERS, SP, ro, ds_), bf),
-            pltpu.VMEM((LAYERS, 3, rp, 2 * cs), bf),
-            pltpu.VMEM((LAYERS, 3, ro, ds_), bf),
+            pltpu.VMEM((LAYERS, rp, 4 * cs), bf),
+            pltpu.VMEM((LAYERS, ro, 2 * ds_), bf),
             pltpu.VMEM((2, T, D), bf),
             pltpu.VMEM((T, D), bf),
             pltpu.VMEM((2, T, C), bf),
@@ -635,28 +731,35 @@
             pltpu.VMEM((T, 2 * ds_), bf),
             pltpu.VMEM((LAYERS, 2, HALO, cs), bf),
             pltpu.VMEM((LAYERS, 2, HALO, cs), bf),
-            pltpu.VMEM((T, 128), f32),
+            pltpu.VMEM((2, T, 128), f32),
             pltpu.VMEM((2, 8, T), f32),
-            pltpu.VMEM((2, S, 8, T), f32),
+            pltpu.VMEM((2, 2 * X, 8, T), f32),
+            pltpu.VMEM((2, 2, 8, T), f32),
+            pltpu.VMEM((LAYERS, HALO, cs), bf),
             pltpu.VMEM((2, T, 128), f32),
             pltpu.VMEM((2, T, 128), jnp.int32),
             pltpu.VMEM((HALO, 128), jnp.int32),
             dma((parts,)),
-            dma((parts, 3)),
+            dma((parts,)),
+            dma((parts,)),
             dma((parts, 3)),
             dma((parts, Z, ny)),
-            dma((parts, 7)),
+            dma((parts, 2, 3)),
             dma((parts, Z, ny)),
             dma((2, 3 + 4 * nx)),
+            dma((2, 4 + 4 * nx)),
             dma((2, 3 + 4 * nx)),
-            dma((2, 3 + 4 * nx)),
-            dma((2, 3 + 4 * nx)),
-            dma((2, S)),
-            dma((2, S)),
+            dma((2, 4 + 4 * nx)),
+            dma((2, 2 * X)),
+            dma((2, 2 * X)),
+            dma((2,)),
+            dma((2, 2)),
+            dma((LAYERS,)),
+            dma((LAYERS,)),
             dma((LAYERS, 2)),
             dma((LAYERS, 2)),
             dma((3,)),
-            dma((4,)),
+            dma((5,)),
         ],
         compiler_params=pltpu.CompilerParams(has_side_effects=True, vmem_limit_bytes=60 << 20),
         name="stack",

time: 336 us -> 324 us (0.964)
  Pallas kernels: 330 us -> 320 us
    pallas_call x1, Pallas kernels: 330 us -> 320 us  [per_device(): pl.pallas_call(functools.partial(kernel, dims), out_shape=jax.ShapeDtypeS...]
where the time goes in v2:
time: 324 us
  Pallas kernels  320 us (99%)
  local copies, waits for them, and re-layouts  3.54 us (1%)
    pallas_call x1, Pallas kernels, per_device(): pl.pallas_call(functools.partial(kernel, dims), out_shape=jax.ShapeDtypeS...  320 us

profile of v2, /device:TPU:0, one launch (start us, length us, event | category | flops | bytes accessed | tf_op | source)
XLA Modules:
  0.0 323.9 jit_solution(14179922299238322312)
XLA Ops:
  0.0 1.5 broadcast_in_dim.2.docs
  1.5 320.3 %stack.1 = bf16[384,1024]{1,0:T(8,128)(2,1)} custom-call(bf16[384,1024]{1,0:T(8,128)(2,1)} %hid.1, s32[384,128]{1,0:T(8,128)} %broadcast_in_dim.2.docs, f32[3,4096]{1,0:T(4,128)} %ngain.1, bf16[3,512,512]{2,1,0:T(8,128)(2,1)} %wv.1, bf16[3,512,512]{2,1,0:T(8,128)(2,1)} %wg.1, f32[3,31,512]{2,1,0:T(8,128)} %taps.1, f32[3,512]{1,0:T(4,128)} %cbias.1, ...), custom_call_target="tpu_custom_call" | custom-call | tf_op jit(solution)/shard_map/stack/pallas_call | solution.py:713
  321.8 2.1 copy.12

commit v3 on v2

--- a/solution.py
+++ b/solution.py
@@ -43,7 +43,6 @@
     glu,
     conv,
     state,
-    final,
     tail,
     halo,
     stat,
@@ -157,18 +156,31 @@
     def staged_ref(q):
         return (stage_o if q % 2 else stage_p).at[q // 2]
 
-    def z_sends(q):
+    def z_sends(q, which=(0, 1, 2)):
         mine = block(q, z * Y + y)
         moves = [
             (1 - h, z_recv.at[q, 0], zn),
             (h, z_recv.at[q, 1 + h], Z - 1 - z),
             (1 - h, z_recv.at[q, 1 + h], Z - 1 - zn),
         ]
-        for i, (half, rsem, zz) in enumerate(moves):
+        for i in which:
+            half, rsem, zz = moves[i]
             for cc in (1, 0):
-                if i == 0 and cc == 0:
+                if i == which[0] and cc == 0 and 1 in which:
                     recv_wait(staged_ref(q), g_recv.at[q])
                 own_send(q, half, mine, z_send.at[q, cc, i], rsem, dev(zz, y, x, cc), cc == 0)
+
+    def z_early(*qs):
+        @pl.when((c == 1) & (inner == 1))
+        def _():
+            for q in qs:
+                z_sends(q, (1,))
+
+    def z_late(*qs):
+        @pl.when((c == 1) & (inner == 1))
+        def _():
+            for q in qs:
+                z_sends(q, (0, 2))
 
     def z_start(*qs, kind=None):
         @pl.when((c == 1) if kind is None else (c == 1) & (inner == kind))
@@ -228,8 +240,8 @@
             send_wait(staged_ref(q), g_send.at[q])
 
     class Gather:
-        def __init__(self, region, recv, sent, source=None):
-            self.region, self.recv, self.sent = region, recv, sent
+        def __init__(self, region, recv, sent, source=None, near=False):
+            self.region, self.recv, self.sent, self.near = region, recv, sent, near
             self.own = region(x, c, z)
             self.source = self.own if source is None else source
 
@@ -262,7 +274,8 @@
             ref = self.region(x, c, zn)
             recv_wait(ref, self.recv.at[1])
             for j in range(1, X):
-                self.forward(ref, 2 + nx + j, dev(z, y, (x + j) % X, c))
+                if not self.near:
+                    self.forward(ref, 2 + nx + j, dev(z, y, (x + j) % X, c))
             self.forward(ref, 2, partner)
 
         def third(self):
@@ -271,6 +284,16 @@
                 recv_wait(ref, self.recv.at[2 + j])
                 self.forward(ref, 2 + 2 * nx + j, partner)
 
+        def beyond(self):
+            @pl.when(c == 0)
+            def _():
+                for j in range(1, X):
+                    recv_wait(self.region(self.xs(j), 1, z), self.recv.at[2 + 2 * nx + j])
+                    for cc in range(2):
+                        ref = self.region(self.xs(j), cc, z)
+                        send(ref, ref, self.sent.at[2 + 4 * nx + 2 * j + cc], self.recv.at[2 + nx + j],
+                             dev(zn, y, x, cc))
+
         def fourth(self):
             for j in range(1, X):
                 ref = self.region(self.xs(j), c, zn)
@@ -284,17 +307,26 @@
 
             recv_wait(self.region(x, 1 - c, zn), self.recv.at[2])
             for j in range(1, X):
-                recv_wait(self.region(self.xs(j), 1 - c, z), self.recv.at[2 + 2 * nx + j])
+                if self.near:
+                    @pl.when(c == 1)
+                    def _():
+                        recv_wait(self.region(self.xs(j), 0, z), self.recv.at[2 + 2 * nx + j])
+                else:
+                    recv_wait(self.region(self.xs(j), 1 - c, z), self.recv.at[2 + 2 * nx + j])
                 recv_wait(self.region(self.xs(j), 1 - c, zn), self.recv.at[2 + 3 * nx + j])
 
         def drained(self):
             for i in [0] + list(range(2, 3 + 4 * nx)):
-                send_wait(self.own, self.sent.at[i])
+                if not (self.near and 3 + nx <= i < 3 + 2 * nx):
+                    send_wait(self.own, self.sent.at[i])
 
             @pl.when(c == 0)
             def _():
                 send_wait(self.own, self.sent.at[1])
                 send_wait(self.own, self.sent.at[3 + 4 * nx])
+                if self.near:
+                    for i in range(2 * nx):
+                        send_wait(self.own, self.sent.at[4 + 4 * nx + i])
 
     def slot(xx, cc, zz):
         return (xx * 2 + cc) * 2 + 1 - ((zz + 1) // 2) % 2
@@ -307,13 +339,13 @@
             )
         return Gather(
             lambda xx, cc, zz: xg.at[k, :, lanes(slot(xx, cc, zz) * ds_, ds_)],
-            h_recv.at[k], h_send.at[k], state.at[k],
+            h_recv.at[k], h_send.at[k], state.at[k], k == 1 and layer == LAYERS - 1,
         )
 
-    def mixed_gather(k):
+    def mixed_gather(layer, k):
         return Gather(
             lambda xx, cc, zz: mg.at[k, :, lanes(slot(xx, cc, zz) * cs, cs)],
-            m_recv.at[k], m_send.at[k],
+            m_recv.at[k], m_send.at[k], near=k == 1 and layer == LAYERS - 1,
         )
 
     def normalise(layer, k):
@@ -610,27 +642,44 @@
                 return gather
 
         if layer:
+            bulk = [o_now, p_next] if more else [o_now]
+            z_early(*bulk)
             gh[0].second()
             gh[0].third()
-            event2(p_now)
+            if layer == 1:
+                event2(p_now)
+            else:
+
+                @pl.when(inner == 0)
+                def _():
+                    event2(p_now)
+
             event3(p_now)
             start_part(o_now)
             gh[1].third()
+            if not more:
+                gh[1].beyond()
             gh[1].second()
-            z_start(*([o_now, p_next] if more else [o_now]))
+            z_start(*bulk, kind=0)
         for k in range(2):
             if k < len(gh):
                 gh[k].fourth()
                 gh[k].last()
+            if layer and k == 0:
+                z_late(*bulk)
             if layer == 0 and k == 0:
                 for kk in range(2):
                     state[kk] = xg[kk, :, lanes(me * ds_, ds_)]
             normalise(layer, k)
             if k == 0:
                 part_ready(p_now)
-            project_tail(layer, k)
-            tail_send(layer, k)
+            if k:
+                project_tail(layer, k)
+                tail_send(layer, k)
             project(layer, k)
+            if k == 0:
+                tail[layer, k] = glu[k, T : T + HALO, :].astype(jnp.bfloat16)
+                tail_send(layer, k)
             if k < len(gh):
                 gh[k].drained()
             if k == 0:
@@ -640,51 +689,81 @@
                     stats_sent(0)
                     stats_sent(1)
             convolve(layer, k)
-            if k == 0:
+            if k == 0 and layer == 0:
                 event1(o_now)
-                event2(o_now)
+
+                @pl.when(inner == 1)
+                def _():
+                    event2(o_now)
+
         for k in range(2):
             tail_recv(layer, k)
             convolve_first(layer, k)
             if layer:
                 gm[k].drained()
             stats_send(k)
-        event3(o_now)
-        if more:
-            start_part(p_next)
+        if layer:
+            event1(o_now)
+            event2(o_now)
+        else:
+
+            @pl.when(inner == 0)
+            def _():
+                event2(o_now)
+
         for k in range(2):
             row_sum(k)
-        gm = [mixed_gather(k) for k in range(2)]
+        gm = [mixed_gather(layer, k) for k in range(2)]
         for k in range(2):
             mix(layer, k)
             gm[k].first()
             gm[k].across()
+        event3(o_now)
         if more:
-            event1(p_next)
+            start_part(p_next)
+            if layer == 0:
+                event1(p_next)
+            else:
+
+                @pl.when(inner == 1)
+                def _():
+                    event1(p_next)
+
         gm[0].third()
         gm[0].second()
         gm[1].third()
+        if not more:
+            gm[1].beyond()
         gm[1].second()
         first = mixed_out(0)
+        if more and layer:
+
+            @pl.when(inner == 1)
+            def _():
+                event2(p_next)
+
+            @pl.when(inner == 0)
+            def _():
+                event1(p_next)
+
         gh = [first, mixed_out(1)]
 
     for k in range(2):
         gm[k].drained()
         stats_sent(k)
     docs_sent()
-    half = final.at[:, lanes(h * ds_, ds_)]
+    half = out.at[:, lanes(h * ds_, ds_)]
     send(state.at[1 - ko], half, f_sem.at[1], f_sem.at[2], zpeer)
-    final[:, lanes(h * ds_, ds_)] = state[ko]
+    done = pltpu.make_async_copy(state.at[ko], half, f_sem.at[0])
+    done.start()
     for layer in range(LAYERS):
         for k in range(2):
             tail_sent(layer, k)
     for q in range(parts):
         part_sent(q)
     send_wait(half, f_sem.at[1])
-    recv_wait(final.at[:, lanes((1 - h) * ds_, ds_)], f_sem.at[2])
-    done = pltpu.make_async_copy(final, out, f_sem.at[0])
-    done.start()
     done.wait()
+    recv_wait(out.at[:, lanes((1 - h) * ds_, ds_)], f_sem.at[2])
 
 
 def per_device(
@@ -728,7 +807,6 @@
             pltpu.VMEM((2, T + HALO, cs), f32),
             pltpu.VMEM((2, T, cs), f32),
             pltpu.VMEM((2, T, ds_), bf),
-            pltpu.VMEM((T, 2 * ds_), bf),
             pltpu.VMEM((LAYERS, 2, HALO, cs), bf),
             pltpu.VMEM((LAYERS, 2, HALO, cs), bf),
             pltpu.VMEM((2, T, 128), f32),
@@ -747,9 +825,9 @@
             dma((parts, 2, 3)),
             dma((parts, Z, ny)),
             dma((2, 3 + 4 * nx)),
-            dma((2, 4 + 4 * nx)),
+            dma((2, 4 + 6 * nx)),
             dma((2, 3 + 4 * nx)),
-            dma((2, 4 + 4 * nx)),
+            dma((2, 4 + 6 * nx)),
             dma((2, 2 * X)),
             dma((2, 2 * X)),
             dma((2,)),

time: 324 us -> 317 us (0.978)
  Pallas kernels: 320 us -> 313 us
    pallas_call x1, Pallas kernels: 320 us -> 313 us  [per_device(): pl.pallas_call(functools.partial(kernel, dims), out_shape=jax.ShapeDtypeS...]
where the time goes in v3:
time: 317 us
  Pallas kernels  313 us (99%)
  local copies, waits for them, and re-layouts  3.54 us (1%)
    pallas_call x1, Pallas kernels, per_device(): pl.pallas_call(functools.partial(kernel, dims), out_shape=jax.ShapeDtypeS...  313 us

profile of v3, /device:TPU:0, one launch (start us, length us, event | category | flops | bytes accessed | tf_op | source)
XLA Modules:
  0.0 316.6 jit_solution(2997370162737765165)
XLA Ops:
  0.0 1.5 broadcast_in_dim.2.docs
  1.5 313.1 %stack.1 = bf16[384,1024]{1,0:T(8,128)(2,1)} custom-call(bf16[384,1024]{1,0:T(8,128)(2,1)} %hid.1, s32[384,128]{1,0:T(8,128)} %broadcast_in_dim.2.docs, f32[3,4096]{1,0:T(4,128)} %ngain.1, bf16[3,512,512]{2,1,0:T(8,128)(2,1)} %wv.1, bf16[3,512,512]{2,1,0:T(8,128)(2,1)} %wg.1, f32[3,31,512]{2,1,0:T(8,128)} %taps.1, f32[3,512]{1,0:T(4,128)} %cbias.1, ...), custom_call_target="tpu_custom_call" | custom-call | tf_op jit(solution)/shard_map/stack/pallas_call | solution.py:792
  314.6 2.1 copy.12

commit v4 on v3

--- a/solution.py
+++ b/solution.py
@@ -384,16 +384,6 @@
             r = (v * jax.nn.sigmoid(g)).astype(jnp.bfloat16)
             glu[k, pl.ds(pl.multiple_of(i * HALO + HALO, HALO), HALO), :] = r.astype(jnp.float32)
 
-    def project_tail(layer, k):
-        rows = slice(T - HALO, T)
-
-        def step(b, acc):
-            lhs = xn[rows, lanes(b * (D // (Z * Y)), D // (Z * Y))]
-            return acc + jnp.dot(lhs, wp_buf[layer, b], preferred_element_type=jnp.float32)
-
-        both = lax.fori_loop(0, Z * Y, step, jnp.zeros((HALO, 2 * cs), jnp.float32))
-        tail[layer, k] = (both[:, 0:cs] * jax.nn.sigmoid(both[:, cs:])).astype(jnp.bfloat16)
-
     def tail_send(layer, k):
         def go(kk, device):
             send(tail.at[layer, k], halo.at[layer, kk], t_send.at[layer, k], t_recv.at[layer, kk], device)
@@ -673,13 +663,9 @@
             normalise(layer, k)
             if k == 0:
                 part_ready(p_now)
-            if k:
-                project_tail(layer, k)
-                tail_send(layer, k)
             project(layer, k)
-            if k == 0:
-                tail[layer, k] = glu[k, T : T + HALO, :].astype(jnp.bfloat16)
-                tail_send(layer, k)
+            tail[layer, k] = glu[k, T : T + HALO, :].astype(jnp.bfloat16)
+            tail_send(layer, k)
             if k < len(gh):
                 gh[k].drained()
             if k == 0:

time: 317 us -> 314 us (level)
  no operation moved by 1% of the time
where the time goes in v4:
time: 314 us
  Pallas kernels  310 us (99%)
  local copies, waits for them, and re-layouts  3.54 us (1%)
    pallas_call x1, Pallas kernels, per_device(): pl.pallas_call(functools.partial(kernel, dims), out_shape=jax.ShapeDtypeS...  310 us

profile of v4, /device:TPU:0, one launch (start us, length us, event | category | flops | bytes accessed | tf_op | source)
XLA Modules:
  0.0 313.7 jit_solution(10373029261647453936)
XLA Ops:
  0.0 1.5 broadcast_in_dim.2.docs
  1.5 310.1 %stack.1 = bf16[384,1024]{1,0:T(8,128)(2,1)} custom-call(bf16[384,1024]{1,0:T(8,128)(2,1)} %hid.1, s32[384,128]{1,0:T(8,128)} %broadcast_in_dim.2.docs, f32[3,4096]{1,0:T(4,128)} %ngain.1, bf16[3,512,512]{2,1,0:T(8,128)(2,1)} %wv.1, bf16[3,512,512]{2,1,0:T(8,128)(2,1)} %wg.1, f32[3,31,512]{2,1,0:T(8,128)} %taps.1, f32[3,512]{1,0:T(4,128)} %cbias.1, ...), custom_call_target="tpu_custom_call" | custom-call | tf_op jit(solution)/shard_map/stack/pallas_call | solution.py:778
  311.6 2.1 copy.12
